TPU v7x, 32 devices: a whole 2x2x4 slice. The times are simulated.
32 devices in a mesh: sp: 8 (over z, x), tp: 4 (over y, core).
Axes of the slice: x: 2, y: 2, z: 4, core: 2. Of those that a mesh axis runs over, the one named last changes fastest.
Arguments:
- queries: bfloat16 [4096, 3072], P('sp', 'tp'), may hold values from -6 to 6
- latent: bfloat16 [4096, 1024], P('sp'), may hold values from -6 to 6
- rope_key: bfloat16 [4096, 64], P('sp'), may hold values from -6 to 6
- key_weight: bfloat16 [1024, 2048], P(None, 'tp'), as said below
- value_weight: bfloat16 [1024, 2048], P(None, 'tp'), as said below
- log_sums: float32 [16, 4096], P('tp', 'sp'), as said below
- attn_out: bfloat16 [4096, 2048], P('sp', 'tp'), as said below
- out_grad: bfloat16 [4096, 2048], P('sp', 'tp'), may hold values from -6 to 6
Outputs:
- d_queries: bfloat16 [4096, 3072], P('sp', 'tp')
- d_latent: float32 [4096, 1024], P('sp')
- d_rope: float32 [4096, 64], P('sp')
- d_value_weight: float32 [1024, 2048], P('sp', 'tp')
Inputs may be any that keep to these rules, and one draw needn't show every extreme that they name: `key_weight`: independent entries of order one multiplied by 1024^(-1/2). `value_weight`: independent entries of order one multiplied by 1024^(-1/2). log_sums[h, i] is the logarithm of the sum over j <= i of exp(scores[h, i, j]) of the forward pass. attn_out is the forward pass output: head h of row i is the sum over j <= i of exp(scores - log_sums) rounded to bfloat16, times head h of values row j, rounded to bfloat16.
All inputs are finite; a program needn't handle non-finite values.
Results may differ from a plain program's by a relative error of at most 0.018.
Values may be sent and summed in bfloat16 or wider, within the bound.
A program may use at most 192 MiB of HBM per device.

v0:
```python
import jax
import jax.numpy as jnp
from jax import lax
from jax.sharding import PartitionSpec as P

NOPE = 128
ROPE = 64
VDIM = 128


def score_block(
    query_nope,
    query_rope,
    grad_heads,
    lse_rows,
    delta_rows,
    key_heads,
    key_rope,
    value_heads,
    key_first,
):
    score_scale = (NOPE + ROPE) ** (-0.5)
    query_count = query_nope.shape[0]
    key_count = key_heads.shape[0]
    scores = score_scale * (
        jnp.einsum("qhn,khn->hqk", query_nope, key_heads, preferred_element_type=jnp.float32)
        + jnp.einsum("qhr,kr->hqk", query_rope, key_rope, preferred_element_type=jnp.float32)
    )
    query_pos = jnp.arange(query_count, dtype=jnp.int32)
    key_pos = key_first + jnp.arange(key_count, dtype=jnp.int32)
    causal = key_pos[None, :] <= query_pos[:, None]
    attn_probs = jnp.exp(jnp.where(causal[None], scores - lse_rows[:, :, None], -1e30))
    probs_b = attn_probs.astype(jnp.bfloat16)
    value_grad = jnp.einsum("hqk,qhv->khv", probs_b, grad_heads, preferred_element_type=jnp.float32)
    prob_grad = jnp.einsum(
        "qhv,khv->hqk", grad_heads, value_heads, preferred_element_type=jnp.float32
    )
    score_grad = (attn_probs * (prob_grad - delta_rows[:, :, None])).astype(jnp.bfloat16)
    query_grad = score_scale * jnp.concatenate(
        [
            jnp.einsum("hqk,khn->qhn", score_grad, key_heads, preferred_element_type=jnp.float32),
            jnp.einsum("hqk,kr->qhr", score_grad, key_rope, preferred_element_type=jnp.float32),
        ],
        axis=2,
    )
    key_grad = score_scale * jnp.einsum(
        "hqk,qhn->khn", score_grad, query_nope, preferred_element_type=jnp.float32
    )
    rope_grad = score_scale * jnp.einsum(
        "hqk,qhr->kr", score_grad, query_rope, preferred_element_type=jnp.float32
    )
    return (query_grad, key_grad, rope_grad, value_grad)


def keep_state(state_in):
    return state_in


def per_device(queries, latent, rope_key, key_weight, value_weight, log_sums, attn_out, out_grad):
    tok_rows = queries.shape[0]
    head_count = key_weight.shape[1] // NOPE
    head_width = NOPE + ROPE
    first_row = lax.axis_index("sp") * tok_rows
    total_rows = tok_rows * lax.axis_size("sp")
    grad_heads = out_grad.reshape(tok_rows, head_count, VDIM)
    out_heads = attn_out.reshape(tok_rows, head_count, VDIM)
    row_terms = jnp.sum(out_heads.astype(jnp.float32) * grad_heads.astype(jnp.float32), axis=2).T
    lse_all, delta_all = (
        lax.all_gather(log_sums, "sp", axis=1, tiled=True),
        lax.all_gather(row_terms, "sp", axis=1, tiled=True),
    )
    row_count = latent.shape[0]
    key_heads = (
        jnp.dot(latent, key_weight, preferred_element_type=jnp.float32)
        .astype(jnp.bfloat16)
        .reshape(row_count, head_count, NOPE)
    )
    value_heads = (
        jnp.dot(latent, value_weight, preferred_element_type=jnp.float32)
        .astype(jnp.bfloat16)
        .reshape(row_count, head_count, VDIM)
    )
    start_state = (
        jnp.zeros((tok_rows, head_count, NOPE), jnp.float32),
        jnp.zeros((tok_rows, ROPE), jnp.float32),
        jnp.zeros((tok_rows, head_count, VDIM), jnp.float32),
        jnp.zeros((total_rows, head_count * head_width), jnp.float32),
    )
    query_piece = lax.all_gather(queries, "sp", axis=0, tiled=True)
    grad_piece = lax.all_gather(out_grad, "sp", axis=0, tiled=True)
    piece_rows = query_piece.shape[0]

    def compute_piece(state_in):
        piece_heads = query_piece.reshape(piece_rows, head_count, head_width)
        query_grad, key_grad, rope_grad, value_grad = score_block(
            piece_heads[:, :, :NOPE],
            piece_heads[:, :, NOPE:],
            grad_piece.reshape(piece_rows, head_count, VDIM),
            lse_all,
            delta_all,
            key_heads,
            rope_key,
            value_heads,
            first_row,
        )
        query_buffer = query_grad.reshape(piece_rows, head_count * head_width)
        return (key_grad, rope_grad, value_grad, query_buffer)

    key_sum, rope_total, value_sum, query_buffer = lax.cond(
        jnp.int32(0) + piece_rows <= first_row, keep_state, compute_piece, start_state
    )
    query_total = lax.psum_scatter(
        query_buffer.astype(jnp.bfloat16), "sp", scatter_dimension=0, tiled=True
    )
    key_grad_b = key_sum.reshape(tok_rows, head_count * NOPE).astype(jnp.bfloat16)
    value_grad_b = value_sum.reshape(tok_rows, head_count * VDIM).astype(jnp.bfloat16)
    latent_part = jnp.dot(key_grad_b, key_weight.T, preferred_element_type=jnp.float32) + jnp.dot(
        value_grad_b, value_weight.T, preferred_element_type=jnp.float32
    )
    d_latent, d_rope = (
        lax.psum(latent_part.astype(jnp.bfloat16), "tp").astype(jnp.float32),
        lax.psum(rope_total.astype(jnp.bfloat16), "tp").astype(jnp.float32),
    )
    d_value_weight = lax.psum_scatter(
        lax.dot_general(
            latent, value_grad_b, (((0,), (0,)), ((), ())), preferred_element_type=jnp.float32
        ).astype(jnp.bfloat16),
        "sp",
        scatter_dimension=0,
        tiled=True,
    ).astype(jnp.float32)
    return (query_total, d_latent, d_rope, d_value_weight)


def solution(mesh):
    placed = (
        P("sp", "tp"),
        P("sp", None),
        P("sp", None),
        P(None, "tp"),
        P(None, "tp"),
        P("tp", "sp"),
        P("sp", "tp"),
        P("sp", "tp"),
    )
    return jax.shard_map(
        per_device,
        mesh=mesh,
        in_specs=placed,
        out_specs=(P("sp", "tp"), P("sp", None), P("sp", None), P("sp", "tp")),
        check_vma=False,
    )
```

profile of v0, /device:TPU:0, one launch (start us, length us, event | category | flops | bytes accessed | tf_op | source)
XLA Modules:
  0.0 581.1 jit_solution(2930090957411692504)
XLA Ops:
  7.2 0.0 copy-start
  7.2 0.0 copy-start.8
  7.2 0.0 all-gather.5.cloned.1.call-start
  7.2 2.1 copy.42
  9.4 0.0 all-gather.5.cloned.1.call-update
  9.4 0.0 copy-start.7
  9.4 0.0 all-gather.3.cloned.1.call-start
  9.4 2.3 copy.41
  11.7 0.0 all-gather.3.cloned.1.call-update
  11.8 0.0 all-reduce.3.cloned.1.call-start
  11.8 1.3 convert_multiply_fusion
  13.2 0.4 mul.31
  13.5 0.6 reduce_sum.9
  14.2 0.0 copy-done.8
  14.2 33.2 %all_gather.13 = f32[4,4096]{1,0:T(4,128)S(1)} all-gather(f32[4,512]{1,0:T(4,128)S(1)} %copy-done.8), channel_id=1, replica_groups=mesh['sp'=8,'tp'=4] {'sp'}, dimensions={1}, use_global_device_ids=true | all-gather | bytes 73728 | tf_op jit(solution)/shard_map/all_gather | solution.py:69
  47.4 59.8 %all_gather.15 = f32[4,4096]{0,1:T(8,128)S(1)} all-gather(f32[4,512]{0,1:T(8,128)S(1)} %bitcast.72), channel_id=1, replica_groups=mesh['sp'=8,'tp'=4] {'sp'}, dimensions={1}, use_global_device_ids=true | all-gather | bytes 73728 | tf_op jit(solution)/shard_map/all_gather | solution.py:70
  107.2 0.0 copy-done
  107.2 2.7 convolution_convert_fusion.2
  110.0 2.7 convolution_convert_fusion.1
  112.7 9.5 %all-gather.5.cloned.1.call-done = bf16[4096,512]{0,1:T(8,128)(2,1)} async-done(((bf16[512,512]{0,1:T(8,128)(2,1)}), bf16[4096,512]{0,1:T(8,128)(2,1)}) %all-gather.5.cloned.1.call-update) | async-done | bytes 4194320 | tf_op jit(solution)/shard_map/all_gather | solution.py:90
  122.2 101.4 %all-gather.3.cloned.1.call-done = bf16[4096,768]{0,1:T(8,128)(2,1)} async-done(((bf16[512,768]{0,1:T(8,128)(2,1)}), bf16[4096,768]{0,1:T(8,128)(2,1)}) %all-gather.3.cloned.1.call-update) | async-done | bytes 6291472 | tf_op jit(solution)/shard_map/all_gather | solution.py:89
  223.6 0.0 copy-done.7
  223.6 121.5 %conditional.1 = (bf16[512,64]{0,1:T(8,128)(2,1)S(1)}, bf16[4096,768]{0,1:T(8,128)(2,1)}, bf16[512,512]{0,1:T(8,128)(2,1)}, bf16[512,512]{0,1:T(8,128)(2,1)}) conditional(s32[]{:T(128)} %convert_element_type.70, (s32[]{:T(128)}, bf16[4096,768]{0,1:T(8,128)(2,1)}, bf16[512,512]{1,0:T(8,128)(2,1)}, bf16[512,64]{0,1:T(8,128)(2,1)S(1)}, ...), branch_computations={%region_1.2_spmd, %region_2.3_spmd} | conditional | flops 14038138880 | bytes 400494752 | solution.py:109
  223.6 0.6 copy.44
  224.2 2.1 copy.43
  226.3 1.7 iota_compare_fusion
  228.0 17.9 %fusion.6 = f32[4,4096,512]{2,1,0:T(8,128)} fusion(bf16[512,4,128]{0,2,1:T(8,128)(2,1)} %bitcast.68, bf16[4096,4,192]{0,2,1:T(8,128)(2,1)} %bitcast.62), kind=kOutput, calls=%fused_computation.12 | convolution fusion | flops 2147483648 | bytes 38273024 | tf_op jit(solution)/shard_map/cond/branch_0_fun/qhn,khn->hqk/dot_general | solution.py:26
  245.9 27.6 %fusion.3 = f32[4,4096,512]{2,1,0:T(8,128)} fusion(f32[4,4096,512]{2,1,0:T(8,128)} %fusion.6, f32[4,4096]{1,0:T(4,128)S(1)} %get-tuple-element.24, pred[4096,512]{1,0:T(8,128)(4,1)S(1)} %iota_compare_fusion, bf16[4096,4,192]{0,2,1:T(8,128)(2,1)} %bitcast.63, bf16[512,64]{0,1:T(8,128)(2,1)S(1)} %get-tuple-element.41), kind=kOutput, calls=%fused_computation.4 | convolution fusion | flops 1107296256 | bytes 71434240 | tf_op jit(solution)/shard_map/cond/branch_0_fun/qhr,kr->hqk/dot_general | solution.py:27
  273.5 0.0 copy-start.5
  273.5 15.0 %fusion.19 = bf16[4,512,128]{1,2,0:T(8,128)(2,1)} fusion(bf16[4096,4,128]{0,2,1:T(8,128)(2,1)} %bitcast.66, f32[4,4096,512]{2,1,0:T(8,128)} %fusion.3), kind=kOutput, calls=%fused_computation.21 | convolution fusion | flops 2156134400 | bytes 38273024 | tf_op jit(solution)/shard_map/cond/branch_0_fun/hqk,qhv->khv/dot_general | solution.py:34
  288.6 0.0 copy-done.5
  288.6 19.1 %multiply_convert_fusion = bf16[4,4096,512]{2,1,0:T(8,128)(2,1)} fusion(f32[4,4096,512]{2,1,0:T(8,128)} %fusion.3, f32[4,4096]{1,0:T(4,128)S(1)} %copy.44, bf16[4096,4,128]{0,2,1:T(8,128)(2,1)} %bitcast.67, bf16[512,512]{1,0:T(8,128)(2,1)S(1)} %copy-done.5), kind=kOutput, calls=%fused_computation.5 | convolution fusion | flops 2172649472 | bytes 55115776 | tf_op jit(solution)/shard_map/cond/branch_0_fun/qhv,khv->hqk/dot_general | solution.py:35
  307.7 0.0 copy-start.1
  307.7 9.5 %fusion.25 = bf16[512,64]{0,1:T(8,128)(2,1)S(1)} fusion(bf16[4,4096,512]{2,1,0:T(8,128)(2,1)} %multiply_convert_fusion, bf16[4096,4,192]{0,2,1:T(8,128)(2,1)} %bitcast.64), kind=kOutput, calls=%fused_computation.23 | convolution fusion | flops 1073807360 | bytes 18939904 | tf_op jit(solution)/shard_map/cond/branch_0_fun/hqk,qhr->kr/dot_general | solution.py:49
  317.3 1.6 copy-done.1
  318.9 5.3 fusion.16
  324.2 0.0 copy-start.3
  324.2 7.1 %convolution_bitcast_fusion.1 = f32[4096,4,64]{0,2,1:T(8,128)} fusion(bf16[4,4096,512]{2,1,0:T(8,128)(2,1)S(1)} %copy-done.1, bf16[512,64]{0,1:T(8,128)(2,1)S(1)} %get-tuple-element.41), kind=kOutput, calls=%fused_computation.11 | convolution fusion | flops 1073741824 | bytes 21037056 | tf_op jit(solution)/shard_map/cond/branch_0_fun/hqk,kr->qhr/dot_general | solution.py:42
  331.3 0.0 copy-done.3
  331.3 0.0 copy-start.2
  331.3 9.2 %convolution_bitcast_fusion = f32[4096,4,128]{0,2,1:T(8,128)S(1)} fusion(bf16[4,4096,512]{2,1,0:T(8,128)(2,1)} %multiply_convert_fusion, bf16[512,4,128]{0,2,1:T(8,128)(2,1)S(1)} %bitcast.69), kind=kOutput, calls=%fused_computation.10 | convolution fusion | flops 2147483648 | bytes 25690112 | tf_op jit(solution)/shard_map/cond/branch_0_fun/hqk,khn->qhn/dot_general | solution.py:41
  340.5 0.0 copy-done.2
  340.5 4.5 maximum_multiply_fusion
  345.0 0.0 copy-start.6
  345.1 0.0 copy-start.4
  345.1 2.2 fusion.33
  347.3 3.2 add_convert_fusion
  350.4 0.0 copy-done.6
  350.4 0.0 all-reduce.3.cloned.1.call-update
  350.4 0.0 reduce-scatter.7.cloned.1.call-start
  350.5 0.0 copy-done.4
  350.5 0.7 fusion.32
  351.2 1.3 copy.51
  352.5 0.0 reduce-scatter.7.cloned.1.call-update
  352.6 0.0 reduce-scatter.5.cloned.1.call-start
  352.6 8.7 %copy.45 = bf16[4096,768]{1,0:T(8,128)(2,1)} copy(bf16[4096,768]{0,1:T(8,128)(2,1)} %get-tuple-element.36) | data formatting | bytes 12582912 | tf_op jit(solution)/shard_map/cond | solution.py:109
  361.3 0.0 reduce-scatter.5.cloned.1.call-update
  361.3 24.4 %all-reduce.3.cloned.1.call-done = (bf16[512,1024]{1,0:T(8,128)(2,1)}, bf16[512,64]{0,1:T(8,128)(2,1)}) async-done(((bf16[512,1024]{1,0:T(8,128)(2,1)}, bf16[512,64]{0,1:T(8,128)(2,1)}), (bf16[512,1024]{1,0:T(8,128)(2,1)}, bf16[512,64]{0,1:T(8,128)(2,1)})) %all-reduce.3.cloned.1.call-update) | async-done | bytes 1114128 | tf_op jit(solution)/shard_map/psum | solution.py:121
  385.7 1.5 convert_element_type.79
  387.2 2.8 convert_element_type.77
  390.0 63.6 %reduce-scatter.7.cloned.1.call-done = bf16[128,512]{1,0:T(8,128)(2,1)} async-done(((bf16[1024,512]{1,0:T(8,128)(2,1)}), bf16[128,512]{1,0:T(8,128)(2,1)}) %reduce-scatter.7.cloned.1.call-update) | async-done | bytes 131088
  453.6 1.0 copy.52
  454.6 0.8 copy.46
  455.4 119.1 %reduce-scatter.5.cloned.1.call-done = bf16[512,768]{1,0:T(8,128)(2,1)} async-done(((bf16[4096,768]{1,0:T(8,128)(2,1)}), bf16[512,768]{1,0:T(8,128)(2,1)}) %reduce-scatter.5.cloned.1.call-update) | async-done | bytes 786448 | tf_op jit(solution)/shard_map/reduce_scatter | solution.py:112
  (1 shorter events, 0.0 us)
Async XLA Ops:
  7.2 100.1 %copy-start = (bf16[512,1024]{1,0:T(8,128)(2,1)S(1)}, bf16[512,1024]{1,0:T(8,128)(2,1)}, u32[]{:S(2)}) copy-start(bf16[512,1024]{1,0:T(8,128)(2,1)} %param.11) | copy-start | bytes 3145732
  7.2 7.0 %copy-start.8 = (f32[4,512]{1,0:T(4,128)S(1)}, f32[4,512]{1,0:T(4,128)}, u32[]{:S(2)}) copy-start(f32[4,512]{1,0:T(4,128)} %param.15) | copy-start | bytes 24580
  7.2 115.0 %all-gather.5.cloned.1.call-start = ((), (), s32[]{:S(2)}) async-start(), calls=%async_computation.3 | async-start | bytes 4718592 | tf_op jit(solution)/shard_map/all_gather | solution.py:90
  9.4 214.2 %copy-start.7 = (bf16[512,64]{0,1:T(8,128)(2,1)S(1)}, bf16[512,64]{0,1:T(8,128)(2,1)}, u32[]{:S(2)}) copy-start(bf16[512,64]{0,1:T(8,128)(2,1)} %param.12) | copy-start | bytes 196612
  9.4 214.2 %all-gather.3.cloned.1.call-start = ((), (), s32[]{:S(2)}) async-start(), calls=%async_computation.2 | async-start | bytes 7077888 | tf_op jit(solution)/shard_map/all_gather | solution.py:89
  11.8 373.9 %all-reduce.3.cloned.1.call-start = ((), (), s32[]{:S(2)}) async-start(), calls=%async_computation.6 | async-start | bytes 2228224 | tf_op jit(solution)/shard_map/psum | solution.py:121
  273.5 15.0 %copy-start.5 = (bf16[512,512]{1,0:T(8,128)(2,1)S(1)}, bf16[512,512]{1,0:T(8,128)(2,1)}, u32[]{:S(2)}) copy-start(bf16[512,512]{1,0:T(8,128)(2,1)} %get-tuple-element.26) | copy-start | bytes 1572868 | tf_op jit(solution)/shard_map/cond
  307.7 11.2 %copy-start.1 = (bf16[4,4096,512]{2,1,0:T(8,128)(2,1)S(1)}, bf16[4,4096,512]{2,1,0:T(8,128)(2,1)}, u32[]{:S(2)}) copy-start(bf16[4,4096,512]{2,1,0:T(8,128)(2,1)} %multiply_convert_fusion) | copy-start | bytes 50331652 | tf_op jit(solution)/shard_map/cond
  324.2 7.1 %copy-start.3 = (bf16[512,512]{0,1:T(8,128)(2,1)S(1)}, bf16[512,512]{0,1:T(8,128)(2,1)}, u32[]{:S(2)}) copy-start(bf16[512,512]{0,1:T(8,128)(2,1)} %copy.43) | copy-start | bytes 1572868 | tf_op jit(solution)/shard_map/cond
  331.3 9.2 %copy-start.2 = (f32[4096,4,64]{0,2,1:T(8,128)S(1)}, f32[4096,4,64]{0,2,1:T(8,128)}, u32[]{:S(2)}) copy-start(f32[4096,4,64]{0,2,1:T(8,128)} %convolution_bitcast_fusion.1) | copy-start | bytes 12582916 | tf_op jit(solution)/shard_map/cond
  345.0 5.4 copy-start.6
  345.1 5.4 copy-start.4
  350.4 103.1 %reduce-scatter.7.cloned.1.call-start = ((), (), s32[]{:S(2)}) async-start(), calls=%async_computation.5 | async-start | bytes 1179648
  352.6 222.0 %reduce-scatter.5.cloned.1.call-start = ((), (), s32[]{:S(2)}) async-start(), calls=%async_computation.4 | async-start | bytes 7077888 | tf_op jit(solution)/shard_map/reduce_scatter | solution.py:112
Sparse Core Ops, SparseCore 0:
  10.0 112.0 all-gather.4
  124.8 98.7 all-gather.2
  350.6 35.0 all-reduce.2
  388.9 64.5 reduce-scatter.6
  457.6 116.9 reduce-scatter.4
where the time goes:
time: 582 us; the launch traced here: 581 us
  waiting for transfers between devices  318 us (55%)
  matrix products  122 us (21%)
  blocking collectives  93.1 us (16%)
  local copies, waits for them, and re-layouts  20.9 us (4%)
  between operations  13.9 us (2%)
  other arithmetic  12.5 us (2%)
    reduce_scatter x1, waiting for transfers between devices, per_device(): lax.psum_scatter(query_buffer.astype(jnp.bfloat16), 'sp', scatter_dimensi...  119 us
    all_gather x1, waiting for transfers between devices, per_device(): query_piece = lax.all_gather(queries, 'sp', axis=0, tiled=True)  101 us
    unnamed x6, waiting for transfers between devices  63.7 us
    all_gather x1, blocking collectives, per_device(): lax.all_gather(row_terms, 'sp', axis=1, tiled=True)  59.8 us
    all_gather x1, blocking collectives, per_device(): lax.all_gather(log_sums, 'sp', axis=1, tiled=True)  33.2 us
    dot_general x1, matrix products, score_block(): jnp.einsum('qhr,kr->hqk', query_rope, key_rope, preferred_element_type=jn...  27.6 us
    psum x1, waiting for transfers between devices, per_device(): lax.psum(latent_part.astype(jnp.bfloat16), 'tp').astype(jnp.float32)  24.4 us
    dot_general x1, matrix products, score_block(): jnp.einsum('qhv,khv->hqk', grad_heads, value_heads, preferred_element_typ...  19.1 us
  transfers between devices with their start and end apart: 5, of which 5 were waited for; matrix products, arithmetic and copies ran while one was open for 5% of the time, Pallas kernels for 0%

commit v1 on v0

--- a/solution.py
+++ b/solution.py
@@ -67,7 +67,7 @@
     row_terms = jnp.sum(out_heads.astype(jnp.float32) * grad_heads.astype(jnp.float32), axis=2).T
     lse_all, delta_all = (
         lax.all_gather(log_sums, "sp", axis=1, tiled=True),
-        lax.all_gather(row_terms, "sp", axis=1, tiled=True),
+        jnp.concatenate(lax.all_gather(row_terms, "sp"), axis=1),
     )
     row_count = latent.shape[0]
     key_heads = (

time: 582 us -> 546 us (0.938)
  blocking collectives: 93.1 us -> 65 us
    all_gather x1, blocking collectives: 59.8 us -> 31.7 us  [per_device(): lax.all_gather(row_terms, 'sp')]
where the time goes in v1:
time: 546 us
  waiting for transfers between devices  313 us (57%)
  matrix products  122 us (22%)
  blocking collectives  65 us (12%)
  local copies, waits for them, and re-layouts  19.4 us (4%)
  between operations  13.9 us (3%)
  other arithmetic  12.5 us (2%)
    reduce_scatter x1, waiting for transfers between devices, per_device(): lax.psum_scatter(query_buffer.astype(jnp.bfloat16), 'sp', scatter_dimensi...  119 us
    all_gather x1, waiting for transfers between devices, per_device(): query_piece = lax.all_gather(queries, 'sp', axis=0, tiled=True)  100 us
    unnamed x6, waiting for transfers between devices  63.7 us
    all_gather x1, blocking collectives, per_device(): lax.all_gather(log_sums, 'sp', axis=1, tiled=True)  33.2 us
    all_gather x1, blocking collectives, per_device(): lax.all_gather(row_terms, 'sp')  31.7 us
    dot_general x1, matrix products, score_block(): jnp.einsum('qhr,kr->hqk', query_rope, key_rope, preferred_element_type=jn...  27.6 us
    psum x1, waiting for transfers between devices, per_device(): lax.psum(latent_part.astype(jnp.bfloat16), 'tp').astype(jnp.float32)  24.4 us
    dot_general x1, matrix products, score_block(): jnp.einsum('qhv,khv->hqk', grad_heads, value_heads, preferred_element_typ...  19.1 us
  transfers between devices with their start and end apart: 5, of which 5 were waited for; matrix products, arithmetic and copies ran while one was open for 5% of the time, Pallas kernels for 0%

profile of v1, /device:TPU:0, one launch (start us, length us, event | category | flops | bytes accessed | tf_op | source)
XLA Modules:
  0.0 545.8 jit_solution(6912787523960520765)
XLA Ops:
  7.2 0.0 copy-start
  7.2 0.0 copy-start.8
  7.2 0.0 copy-start.7
  7.2 0.0 all-gather.7.cloned.1.call-start
  7.2 2.1 copy.42
  9.4 0.0 all-gather.7.cloned.1.call-update
  9.4 0.0 all-gather.5.cloned.1.call-start
  9.4 2.3 copy.41
  11.7 0.0 all-gather.5.cloned.1.call-update
  11.8 0.0 all-reduce.3.cloned.1.call-start
  11.8 1.3 convert_multiply_fusion
  13.2 0.4 mul.31
  13.5 0.6 reduce_sum.9
  14.2 0.1 copy.43
  14.3 0.0 copy-done.8
  14.3 33.2 %all_gather.16 = f32[4,4096]{1,0:T(4,128)S(1)} all-gather(f32[4,512]{1,0:T(4,128)S(1)} %copy-done.8), channel_id=1, replica_groups=mesh['sp'=8,'tp'=4] {'sp'}, dimensions={1}, use_global_device_ids=true | all-gather | bytes 73728 | tf_op jit(solution)/shard_map/all_gather | solution.py:69
  47.5 31.7 %all-gather.1 = f32[8,4,512]{2,1,0:T(4,128)S(1)} all-gather(f32[1,4,512]{2,1,0:T(4,128)S(1)} %copy.43), channel_id=2, replica_groups=mesh['sp'=8,'tp'=4] {'sp'}, dimensions={0}, use_global_device_ids=true | all-gather | bytes 73728 | tf_op jit(solution)/shard_map/all_gather | solution.py:70
  79.2 0.0 copy-done
  79.2 1.9 convolution_convert_fusion.2
  81.2 2.7 convolution_convert_fusion.1
  83.9 5.5 %all-gather.7.cloned.1.call-done = bf16[4096,512]{0,1:T(8,128)(2,1)} async-done(((bf16[512,512]{0,1:T(8,128)(2,1)}), bf16[4096,512]{0,1:T(8,128)(2,1)}) %all-gather.7.cloned.1.call-update) | async-done | bytes 4194320 | tf_op jit(solution)/shard_map/all_gather | solution.py:90
  89.4 100.5 %all-gather.5.cloned.1.call-done = bf16[4096,768]{0,1:T(8,128)(2,1)} async-done(((bf16[512,768]{0,1:T(8,128)(2,1)}), bf16[4096,768]{0,1:T(8,128)(2,1)}) %all-gather.5.cloned.1.call-update) | async-done | bytes 6291472 | tf_op jit(solution)/shard_map/all_gather | solution.py:89
  189.9 0.0 copy-done.7
  189.9 119.8 %conditional.1 = (bf16[512,64]{0,1:T(8,128)(2,1)S(1)}, bf16[4096,768]{0,1:T(8,128)(2,1)}, bf16[512,512]{0,1:T(8,128)(2,1)}, bf16[512,512]{0,1:T(8,128)(2,1)}) conditional(s32[]{:T(128)} %convert_element_type.70, (s32[]{:T(128)}, bf16[4096,768]{0,1:T(8,128)(2,1)}, bf16[512,512]{1,0:T(8,128)(2,1)S(1)}, bf16[512,64]{0,1:T(8,128)(2,1)S(1)}, ...), branch_computations={%region_1.2_spmd, %region_2.3_spmd} | conditional | flops 14038138880 | bytes 400363680 | solution.py:109
  189.9 1.0 copy.44
  190.9 1.7 iota_compare_fusion
  192.6 17.9 %fusion.6 = f32[4,4096,512]{2,1,0:T(8,128)} fusion(bf16[512,4,128]{0,2,1:T(8,128)(2,1)} %bitcast.72, bf16[4096,4,192]{0,2,1:T(8,128)(2,1)} %bitcast.66), kind=kOutput, calls=%fused_computation.12 | convolution fusion | flops 2147483648 | bytes 38273024 | tf_op jit(solution)/shard_map/cond/branch_0_fun/qhn,khn->hqk/dot_general | solution.py:26
  210.5 27.6 %fusion.3 = f32[4,4096,512]{2,1,0:T(8,128)} fusion(f32[4,4096,512]{2,1,0:T(8,128)} %fusion.6, f32[4,4096]{1,0:T(4,128)S(1)} %get-tuple-element.24, pred[4096,512]{1,0:T(8,128)(4,1)S(1)} %iota_compare_fusion, bf16[4096,4,192]{0,2,1:T(8,128)(2,1)} %bitcast.67, bf16[512,64]{0,1:T(8,128)(2,1)S(1)} %get-tuple-element.41), kind=kOutput, calls=%fused_computation.4 | convolution fusion | flops 1107296256 | bytes 71434240 | tf_op jit(solution)/shard_map/cond/branch_0_fun/qhr,kr->hqk/dot_general | solution.py:27
  238.1 0.0 copy-start.5
  238.1 15.0 %fusion.19 = bf16[4,512,128]{1,2,0:T(8,128)(2,1)} fusion(bf16[4096,4,128]{0,2,1:T(8,128)(2,1)} %bitcast.70, f32[4,4096,512]{2,1,0:T(8,128)} %fusion.3), kind=kOutput, calls=%fused_computation.21 | convolution fusion | flops 2156134400 | bytes 38273024 | tf_op jit(solution)/shard_map/cond/branch_0_fun/hqk,qhv->khv/dot_general | solution.py:34
  253.1 0.0 copy-done.5
  253.1 19.1 %multiply_convert_fusion = bf16[4,4096,512]{2,1,0:T(8,128)(2,1)} fusion(f32[4,4096,512]{2,1,0:T(8,128)} %fusion.3, f32[4,4096]{1,0:T(4,128)S(1)} %bitcast.77, bf16[4096,4,128]{0,2,1:T(8,128)(2,1)} %bitcast.71, bf16[512,512]{1,0:T(8,128)(2,1)S(1)} %copy-done.5), kind=kOutput, calls=%fused_computation.5 | convolution fusion | flops 2172649472 | bytes 55115776 | tf_op jit(solution)/shard_map/cond/branch_0_fun/qhv,khv->hqk/dot_general | solution.py:35
  272.3 0.0 copy-start.1
  272.3 9.5 %fusion.25 = bf16[512,64]{0,1:T(8,128)(2,1)S(1)} fusion(bf16[4,4096,512]{2,1,0:T(8,128)(2,1)} %multiply_convert_fusion, bf16[4096,4,192]{0,2,1:T(8,128)(2,1)} %bitcast.68), kind=kOutput, calls=%fused_computation.23 | convolution fusion | flops 1073807360 | bytes 18939904 | tf_op jit(solution)/shard_map/cond/branch_0_fun/hqk,qhr->kr/dot_general | solution.py:49
  281.8 1.6 copy-done.1
  283.5 5.3 fusion.16
  288.8 0.0 copy-start.3
  288.8 7.1 %convolution_bitcast_fusion.1 = f32[4096,4,64]{0,2,1:T(8,128)} fusion(bf16[4,4096,512]{2,1,0:T(8,128)(2,1)S(1)} %copy-done.1, bf16[512,64]{0,1:T(8,128)(2,1)S(1)} %get-tuple-element.41), kind=kOutput, calls=%fused_computation.11 | convolution fusion | flops 1073741824 | bytes 21037056 | tf_op jit(solution)/shard_map/cond/branch_0_fun/hqk,kr->qhr/dot_general | solution.py:42
  295.9 0.0 copy-done.3
  295.9 0.0 copy-start.2
  295.9 9.2 %convolution_bitcast_fusion = f32[4096,4,128]{0,2,1:T(8,128)S(1)} fusion(bf16[4,4096,512]{2,1,0:T(8,128)(2,1)} %multiply_convert_fusion, bf16[512,4,128]{0,2,1:T(8,128)(2,1)S(1)} %bitcast.73), kind=kOutput, calls=%fused_computation.10 | convolution fusion | flops 2147483648 | bytes 25690112 | tf_op jit(solution)/shard_map/cond/branch_0_fun/hqk,khn->qhn/dot_general | solution.py:41
  305.1 0.0 copy-done.2
  305.1 4.5 maximum_multiply_fusion
  309.6 0.0 copy-start.6
  309.6 0.0 copy-start.4
  309.6 2.2 fusion.33
  311.8 3.2 add_convert_fusion
  315.0 0.0 copy-done.6
  315.0 0.0 all-reduce.3.cloned.1.call-update
  315.0 0.0 reduce-scatter.7.cloned.1.call-start
  315.1 0.0 copy-done.4
  315.1 0.7 fusion.32
  315.8 1.3 copy.52
  317.1 0.0 reduce-scatter.7.cloned.1.call-update
  317.1 0.0 reduce-scatter.5.cloned.1.call-start
  317.2 8.7 %copy.46 = bf16[4096,768]{1,0:T(8,128)(2,1)} copy(bf16[4096,768]{0,1:T(8,128)(2,1)} %get-tuple-element.36) | data formatting | bytes 12582912 | tf_op jit(solution)/shard_map/cond | solution.py:109
  325.9 0.0 reduce-scatter.5.cloned.1.call-update
  325.9 24.4 %all-reduce.3.cloned.1.call-done = (bf16[512,1024]{1,0:T(8,128)(2,1)}, bf16[512,64]{0,1:T(8,128)(2,1)}) async-done(((bf16[512,1024]{1,0:T(8,128)(2,1)}, bf16[512,64]{0,1:T(8,128)(2,1)}), (bf16[512,1024]{1,0:T(8,128)(2,1)}, bf16[512,64]{0,1:T(8,128)(2,1)})) %all-reduce.3.cloned.1.call-update) | async-done | bytes 1114128 | tf_op jit(solution)/shard_map/psum | solution.py:121
  350.3 1.5 convert_element_type.79
  351.8 2.8 convert_element_type.77
  354.6 63.6 %reduce-scatter.7.cloned.1.call-done = bf16[128,512]{1,0:T(8,128)(2,1)} async-done(((bf16[1024,512]{1,0:T(8,128)(2,1)}), bf16[128,512]{1,0:T(8,128)(2,1)}) %reduce-scatter.7.cloned.1.call-update) | async-done | bytes 131088
  418.2 1.0 copy.53
  419.2 0.8 copy.47
  420.0 119.2 %reduce-scatter.5.cloned.1.call-done = bf16[512,768]{1,0:T(8,128)(2,1)} async-done(((bf16[4096,768]{1,0:T(8,128)(2,1)}), bf16[512,768]{1,0:T(8,128)(2,1)}) %reduce-scatter.5.cloned.1.call-update) | async-done | bytes 786448 | tf_op jit(solution)/shard_map/reduce_scatter | solution.py:112
  (1 shorter events, 0.0 us)
Async XLA Ops:
  7.2 72.1 %copy-start = (bf16[512,1024]{1,0:T(8,128)(2,1)S(1)}, bf16[512,1024]{1,0:T(8,128)(2,1)}, u32[]{:S(2)}) copy-start(bf16[512,1024]{1,0:T(8,128)(2,1)} %param.11) | copy-start | bytes 3145732
  7.2 7.1 %copy-start.8 = (f32[4,512]{1,0:T(4,128)S(1)}, f32[4,512]{1,0:T(4,128)}, u32[]{:S(2)}) copy-start(f32[4,512]{1,0:T(4,128)} %param.15) | copy-start | bytes 24580
  7.2 182.7 %copy-start.7 = (bf16[512,64]{0,1:T(8,128)(2,1)S(1)}, bf16[512,64]{0,1:T(8,128)(2,1)}, u32[]{:S(2)}) copy-start(bf16[512,64]{0,1:T(8,128)(2,1)} %param.12) | copy-start | bytes 196612
  7.2 82.2 %all-gather.7.cloned.1.call-start = ((), (), s32[]{:S(2)}) async-start(), calls=%async_computation.3 | async-start | bytes 4718592 | tf_op jit(solution)/shard_map/all_gather | solution.py:90
  9.4 180.5 %all-gather.5.cloned.1.call-start = ((), (), s32[]{:S(2)}) async-start(), calls=%async_computation.2 | async-start | bytes 7077888 | tf_op jit(solution)/shard_map/all_gather | solution.py:89
  11.8 338.5 %all-reduce.3.cloned.1.call-start = ((), (), s32[]{:S(2)}) async-start(), calls=%async_computation.6 | async-start | bytes 2228224 | tf_op jit(solution)/shard_map/psum | solution.py:121
  238.1 15.0 %copy-start.5 = (bf16[512,512]{1,0:T(8,128)(2,1)S(1)}, bf16[512,512]{1,0:T(8,128)(2,1)}, u32[]{:S(2)}) copy-start(bf16[512,512]{1,0:T(8,128)(2,1)} %get-tuple-element.26) | copy-start | bytes 1572868 | tf_op jit(solution)/shard_map/cond
  272.3 11.2 %copy-start.1 = (bf16[4,4096,512]{2,1,0:T(8,128)(2,1)S(1)}, bf16[4,4096,512]{2,1,0:T(8,128)(2,1)}, u32[]{:S(2)}) copy-start(bf16[4,4096,512]{2,1,0:T(8,128)(2,1)} %multiply_convert_fusion) | copy-start | bytes 50331652 | tf_op jit(solution)/shard_map/cond
  288.8 7.1 %copy-start.3 = (bf16[512,512]{0,1:T(8,128)(2,1)S(1)}, bf16[512,512]{0,1:T(8,128)(2,1)}, u32[]{:S(2)}) copy-start(bf16[512,512]{0,1:T(8,128)(2,1)} %copy.44) | copy-start | bytes 1572868 | tf_op jit(solution)/shard_map/cond
  295.9 9.2 %copy-start.2 = (f32[4096,4,64]{0,2,1:T(8,128)S(1)}, f32[4096,4,64]{0,2,1:T(8,128)}, u32[]{:S(2)}) copy-start(f32[4096,4,64]{0,2,1:T(8,128)} %convolution_bitcast_fusion.1) | copy-start | bytes 12582916 | tf_op jit(solution)/shard_map/cond
  309.6 5.4 copy-start.6
  309.6 5.4 copy-start.4
  315.0 103.2 %reduce-scatter.7.cloned.1.call-start = ((), (), s32[]{:S(2)}) async-start(), calls=%async_computation.5 | async-start | bytes 1179648
  317.1 222.1 %reduce-scatter.5.cloned.1.call-start = ((), (), s32[]{:S(2)}) async-start(), calls=%async_computation.4 | async-start | bytes 7077888 | tf_op jit(solution)/shard_map/reduce_scatter | solution.py:112
Sparse Core Ops, SparseCore 0:
  10.6 78.7 all-gather.6
  92.0 97.8 all-gather.4
  315.1 35.1 all-reduce.2
  353.6 64.5 reduce-scatter.6
  422.2 117.0 reduce-scatter.4
